TPU v7x, 32 devices: a whole 2x2x4 slice. The times are simulated.
32 devices in a mesh: tp: 8 (over z, y), dp: 4 (over x, core).
Axes of the slice: x: 2, y: 2, z: 4, core: 2. Of those that a mesh axis runs over, the one named last changes fastest.
Arguments:
- activation_rows: bfloat16 [1024, 4096], P(None, 'dp'), may hold values from -24 to 24
- fresh_spans: int32 [128], P('dp'), may hold values from 1 to 8, 384 in all
- entry_rescale_vector: float32 [2, 4096], P(None, 'dp'), may hold values from 0.1 to 1.9
- probe_kernel: bfloat16 [2, 4096, 4096], P(None, 'dp', 'tp'), may hold values from -0.09375 to 0.09375
- retention_kernel: bfloat16 [2, 4096, 4096], P(None, 'dp', 'tp'), may hold values from -0.09375 to 0.09375
- content_kernel: bfloat16 [2, 4096, 4096], P(None, 'dp', 'tp'), may hold values from -0.09375 to 0.09375
- valve_kernel: bfloat16 [2, 4096, 4096], P(None, 'dp', 'tp'), may hold values from -0.09375 to 0.09375
- retention_minimum: float32 [2, 4096], P(None, 'tp'), may hold values from 0 to 0.99
- extra_attenuation: float32 [2, 1024, 32], P(None, 'dp', 'tp'), may hold values from -0.7 to 0
- channel_rescale_vector: float32 [2, 4096], P(None, 'tp'), may hold values from 0.1 to 1.9
- emission_kernel: bfloat16 [2, 4096, 4096], P(None, 'tp', 'dp'), may hold values from -0.09375 to 0.09375
- memory_grids: float32 [2, 128, 32, 128, 128], P(None, 'dp', 'tp'), may hold values from -0.6 to 0.6
Outputs:
- mixed: bfloat16 [1024, 4096], P(None, 'dp')
- new_states: float32 [2, 128, 32, 128, 128], P(None, 'dp', 'tp')
Inputs may be any that keep to these rules, and one draw needn't show every extreme that they name: `fresh_spans`: each sequence has at least one live slot.
All inputs are finite; a program needn't handle non-finite values. No bound on the sum of `fresh_spans` on one device may be relied on, other than what follows from the above.
Results may differ from a plain program's by a relative error of at most 0.017.
Values may be sent and summed in bfloat16 or wider, within the bound.
A program may use at most 128 MiB of HBM per device.

v0:
```python
import jax
import jax.numpy as jnp
from jax import lax
from jax.sharding import PartitionSpec as P

D = 4096
BLOCKS = 2
EPSILON = 1e-05


def update_tick(
    probe_scores,
    retention_scores,
    content_scores,
    valve_scores,
    minimum_bound,
    spike_ledger,
    attention_multiplier,
    stream_spans,
    memory_grid,
):
    stream_tally = memory_grid.shape[0]
    attention_tally = memory_grid.shape[1]
    key_dim = memory_grid.shape[2]
    value_dim = memory_grid.shape[3]
    position_tally = probe_scores.shape[0] // stream_tally

    def split_heads(array, width):
        return array.astype(jnp.float32).reshape(
            stream_tally, position_tally, attention_tally, width
        )

    queries = jax.nn.silu(split_heads(probe_scores, key_dim))
    forget_in = split_heads(retention_scores, key_dim)
    lower_heads = minimum_bound.reshape(attention_tally, key_dim)
    retention_sigmoid = lower_heads + (1.0 - lower_heads) * jax.nn.sigmoid(forget_in)
    key_vecs = (1.0 - lower_heads) * jax.nn.sigmoid(-forget_in)
    log_attenuation = (
        jnp.log(retention_sigmoid)
        + spike_ledger.reshape(stream_tally, position_tally, attention_tally)[..., None]
    )
    values = split_heads(content_scores, value_dim)
    positions = lax.broadcasted_iota(jnp.int32, (stream_tally, position_tally), 1)
    live_mask = positions < stream_spans[:, None]

    def advance(matrix, inputs):
        query_now, key_now, decay_now, value_now, live_now = inputs
        updated = (
            jnp.exp(decay_now)[..., None] * matrix + key_now[..., None] * value_now[..., None, :]
        )
        matrix = jnp.where(live_now[:, None, None, None], updated, matrix)
        readout = jnp.einsum("shkv,shk->shv", matrix, query_now, precision=lax.Precision.HIGHEST)
        return (matrix, readout)

    ending_emission, readouts = lax.scan(
        advance,
        memory_grid,
        (
            jnp.moveaxis(queries, 1, 0),
            jnp.moveaxis(key_vecs, 1, 0),
            jnp.moveaxis(log_attenuation, 1, 0),
            jnp.moveaxis(values, 1, 0),
            jnp.moveaxis(live_mask, 1, 0),
        ),
    )
    readouts = jnp.moveaxis(readouts, 0, 1)
    normed = readouts * lax.rsqrt(jnp.mean(readouts * readouts, axis=-1, keepdims=True) + EPSILON)
    normed = (
        normed
        * attention_multiplier.reshape(attention_tally, value_dim)
        * jax.nn.silu(split_heads(valve_scores, value_dim))
    )
    normed = normed * live_mask.astype(jnp.float32)[..., None, None]
    return (
        normed.reshape(stream_tally * position_tally, attention_tally * value_dim).astype(
            jnp.bfloat16
        ),
        ending_emission,
    )


def local(
    activation_rows,
    fresh_spans,
    entry_rescale_vector,
    probe_kernel,
    retention_kernel,
    content_kernel,
    valve_kernel,
    retention_minimum,
    extra_attenuation,
    channel_rescale_vector,
    emission_kernel,
    memory_grids,
):
    residual = activation_rows
    own_rows = activation_rows.shape[0] // lax.axis_size("dp")
    finals = []
    for layer_index in range(BLOCKS):
        current = residual.astype(jnp.float32)
        squares = lax.psum(jnp.sum(current * current, axis=1), "dp")
        row_scale = lax.rsqrt(squares / D + EPSILON)
        normed = (current * entry_rescale_vector[layer_index]).astype(jnp.bfloat16)
        weights = (
            probe_kernel[layer_index],
            retention_kernel[layer_index],
            content_kernel[layer_index],
            valve_kernel[layer_index],
        )

        def project():
            return jnp.concatenate(
                [jnp.dot(normed, weight, preferred_element_type=jnp.float32) for weight in weights],
                axis=1,
            )

        summed = lax.psum_scatter(
            project().astype(jnp.bfloat16), "dp", scatter_dimension=0, tiled=True
        ).astype(jnp.float32)
        own_scale = lax.dynamic_slice_in_dim(
            row_scale, lax.axis_index("dp") * own_rows, own_rows, 0
        )
        scaled = (summed * own_scale[:, None]).astype(jnp.bfloat16)
        bounds = [0]
        for weight in weights:
            bounds.append(bounds[-1] + weight.shape[1])
        pieces = [scaled[:, bounds[index] : bounds[index + 1]] for index in range(4)]
        attention_yields, ending_emission = update_tick(
            pieces[0],
            pieces[1],
            pieces[2],
            pieces[3],
            retention_minimum[layer_index],
            extra_attenuation[layer_index],
            channel_rescale_vector[layer_index],
            fresh_spans,
            memory_grids[layer_index],
        )
        finals.append(ending_emission)
        out_weight = emission_kernel[layer_index]
        partial_value = jnp.dot(
            lax.all_gather(attention_yields, "dp", axis=0, tiled=True),
            out_weight,
            preferred_element_type=jnp.float32,
        )
        update = lax.psum(partial_value.astype(jnp.bfloat16), "tp")
        residual = (current + update.astype(jnp.float32)).astype(jnp.bfloat16)
    return (residual, jnp.stack(finals))


def solution(mesh):
    placed = (
        P(None, "dp"),
        P("dp"),
        P(None, "dp"),
        P(None, "dp", "tp"),
        P(None, "dp", "tp"),
        P(None, "dp", "tp"),
        P(None, "dp", "tp"),
        P(None, "tp"),
        P(None, "dp", "tp"),
        P(None, "tp"),
        P(None, "tp", "dp"),
        P(None, "dp", "tp", None, None),
    )
    return jax.shard_map(
        local,
        mesh=mesh,
        in_specs=placed,
        out_specs=(P(None, "dp"), P(None, "dp", "tp", None, None)),
        check_vma=False,
    )
```

profile of v0, /device:TPU:0, one launch (start us, length us, event | category | flops | bytes accessed | tf_op | source)
XLA Modules:
  0.0 776.6 jit_solution(9495806767793799022)
XLA Ops:
  8.1 3.5 convolution_convert_fusion.6
  19.7 8.4 %psum.28 = f32[1024]{0:T(1024)S(1)} all-reduce(f32[1024]{0:T(1024)S(1)} %fusion.7), channel_id=1, replica_groups=mesh['tp'=8,'dp'=4] {'dp'}, use_global_device_ids=true, to_apply=%region_2.0 | all-reduce | flops 1024 | bytes 8192 | tf_op jit(solution)/shard_map/psum | solution.py:101
  28.3 12.2 %slice_bitcast_fusion = (f32[32,4,128,128]{3,2,1,0:T(8,128)}, f32[32,4,128,128]{3,2,1,0:T(8,128)}) fusion(f32[2,32,4,128,128]{4,3,2,1,0:T(8,128)} %param.27), kind=kLoop, calls=%fused_computation.21 | loop fusion | bytes 33554432 | tf_op jit(solution)/shard_map/squeeze | solution.py:137
  40.6 25.1 %reduce-scatter.3.cloned.1.call-done = bf16[256,2048]{0,1:T(8,128)(2,1)} async-done(((bf16[1024,2048]{0,1:T(8,128)(2,1)}), bf16[256,2048]{0,1:T(8,128)(2,1)}) %reduce-scatter.3.cloned.1.call-update) | async-done | bytes 1048592 | tf_op jit(solution)/shard_map/reduce_scatter | solution.py:117
  70.5 183.0 %while.24 = (s32[]{:T(128)}, f32[32,4,128,128]{3,2,1,0:T(8,128)}, f32[8,32,4,128]{3,0,2,1:T(8,128)S(1)}, pred[8,32]{1,0:T(8,128)(4,1)S(1)}, f32[8,32,4,128]{3,0,...) while((s32[]{:T(128)}, f32[32,4,128,128]{3,2,1,0:T(8,128)}, ...), condition=%wide.region_4.5_spmd, body=%wide.region_3.4_spmd.sunk | while | flops 33554432 | bytes 26149088 | solution.py:55
  71.9 10.5 %add_select_fusion.4 = f32[32,4,128,128]{3,2,1,0:T(8,128)} fusion(f32[32,4,128,128]{3,2,1,0:T(8,128)} %get-tuple-element.320, f32[32,4,128]{2,1,0:T(4,128)S(1)} %bitcast.274, f32[32,4,128]{2,1,0:T(4,128)S(1)} %bitcast.275, f32[32,4,128]{2,1,0:T(4,128)S(1)} %exponential_bitcast_fusion.4, pred[32]{0:T(512)(128)(4,1)S(1)} %dynamic-slice_bitcast_fusion.4), kind=kLoop, calls=%fused_computation.clone.1 | loop fusion | flops 8388608 | bytes 16973856 | tf_op jit(solution)/shard_map/while/body/eval_jaxpr/jit(_where)/select_n | solution.py:51
  82.5 9.5 %convolution_bitcast_fusion.4 = f32[1,32,4,128]{3,0,2,1:T(1,128)S(1)} fusion(f32[32,4,128,128]{3,2,1,0:T(8,128)} %add_select_fusion.4, f32[8,32,4,128]{3,0,2,1:T(8,128)S(1)} %get-tuple-element.336, s32[]{:T(128)S(6)} %copy.127), kind=kOutput, calls=%fused_computation.1.clone.1 | convolution fusion | flops 25165824 | bytes 8519684 | tf_op jit(solution)/shard_map/while/body/eval_jaxpr/shkv,shk->shv/dot_general | solution.py:52
  94.8 10.5 %add_select_fusion.4 = f32[32,4,128,128]{3,2,1,0:T(8,128)} fusion(f32[32,4,128,128]{3,2,1,0:T(8,128)} %get-tuple-element.320, f32[32,4,128]{2,1,0:T(4,128)S(1)} %bitcast.274, f32[32,4,128]{2,1,0:T(4,128)S(1)} %bitcast.275, f32[32,4,128]{2,1,0:T(4,128)S(1)} %exponential_bitcast_fusion.4, pred[32]{0:T(512)(128)(4,1)S(1)} %dynamic-slice_bitcast_fusion.4), kind=kLoop, calls=%fused_computation.clone.1 | loop fusion | flops 8388608 | bytes 16973856 | tf_op jit(solution)/shard_map/while/body/eval_jaxpr/jit(_where)/select_n | solution.py:51
  105.4 9.5 %convolution_bitcast_fusion.4 = f32[1,32,4,128]{3,0,2,1:T(1,128)S(1)} fusion(f32[32,4,128,128]{3,2,1,0:T(8,128)} %add_select_fusion.4, f32[8,32,4,128]{3,0,2,1:T(8,128)S(1)} %get-tuple-element.336, s32[]{:T(128)S(6)} %copy.127), kind=kOutput, calls=%fused_computation.1.clone.1 | convolution fusion | flops 25165824 | bytes 8519684 | tf_op jit(solution)/shard_map/while/body/eval_jaxpr/shkv,shk->shv/dot_general | solution.py:52
  117.7 10.5 %add_select_fusion.4 = f32[32,4,128,128]{3,2,1,0:T(8,128)} fusion(f32[32,4,128,128]{3,2,1,0:T(8,128)} %get-tuple-element.320, f32[32,4,128]{2,1,0:T(4,128)S(1)} %bitcast.274, f32[32,4,128]{2,1,0:T(4,128)S(1)} %bitcast.275, f32[32,4,128]{2,1,0:T(4,128)S(1)} %exponential_bitcast_fusion.4, pred[32]{0:T(512)(128)(4,1)S(1)} %dynamic-slice_bitcast_fusion.4), kind=kLoop, calls=%fused_computation.clone.1 | loop fusion | flops 8388608 | bytes 16973856 | tf_op jit(solution)/shard_map/while/body/eval_jaxpr/jit(_where)/select_n | solution.py:51
  128.2 9.5 %convolution_bitcast_fusion.4 = f32[1,32,4,128]{3,0,2,1:T(1,128)S(1)} fusion(f32[32,4,128,128]{3,2,1,0:T(8,128)} %add_select_fusion.4, f32[8,32,4,128]{3,0,2,1:T(8,128)S(1)} %get-tuple-element.336, s32[]{:T(128)S(6)} %copy.127), kind=kOutput, calls=%fused_computation.1.clone.1 | convolution fusion | flops 25165824 | bytes 8519684 | tf_op jit(solution)/shard_map/while/body/eval_jaxpr/shkv,shk->shv/dot_general | solution.py:52
  140.6 10.5 %add_select_fusion.4 = f32[32,4,128,128]{3,2,1,0:T(8,128)} fusion(f32[32,4,128,128]{3,2,1,0:T(8,128)} %get-tuple-element.320, f32[32,4,128]{2,1,0:T(4,128)S(1)} %bitcast.274, f32[32,4,128]{2,1,0:T(4,128)S(1)} %bitcast.275, f32[32,4,128]{2,1,0:T(4,128)S(1)} %exponential_bitcast_fusion.4, pred[32]{0:T(512)(128)(4,1)S(1)} %dynamic-slice_bitcast_fusion.4), kind=kLoop, calls=%fused_computation.clone.1 | loop fusion | flops 8388608 | bytes 16973856 | tf_op jit(solution)/shard_map/while/body/eval_jaxpr/jit(_where)/select_n | solution.py:51
  151.1 9.5 %convolution_bitcast_fusion.4 = f32[1,32,4,128]{3,0,2,1:T(1,128)S(1)} fusion(f32[32,4,128,128]{3,2,1,0:T(8,128)} %add_select_fusion.4, f32[8,32,4,128]{3,0,2,1:T(8,128)S(1)} %get-tuple-element.336, s32[]{:T(128)S(6)} %copy.127), kind=kOutput, calls=%fused_computation.1.clone.1 | convolution fusion | flops 25165824 | bytes 8519684 | tf_op jit(solution)/shard_map/while/body/eval_jaxpr/shkv,shk->shv/dot_general | solution.py:52
  163.5 10.5 %add_select_fusion.4 = f32[32,4,128,128]{3,2,1,0:T(8,128)} fusion(f32[32,4,128,128]{3,2,1,0:T(8,128)} %get-tuple-element.320, f32[32,4,128]{2,1,0:T(4,128)S(1)} %bitcast.274, f32[32,4,128]{2,1,0:T(4,128)S(1)} %bitcast.275, f32[32,4,128]{2,1,0:T(4,128)S(1)} %exponential_bitcast_fusion.4, pred[32]{0:T(512)(128)(4,1)S(1)} %dynamic-slice_bitcast_fusion.4), kind=kLoop, calls=%fused_computation.clone.1 | loop fusion | flops 8388608 | bytes 16973856 | tf_op jit(solution)/shard_map/while/body/eval_jaxpr/jit(_where)/select_n | solution.py:51
  174.0 9.5 %convolution_bitcast_fusion.4 = f32[1,32,4,128]{3,0,2,1:T(1,128)S(1)} fusion(f32[32,4,128,128]{3,2,1,0:T(8,128)} %add_select_fusion.4, f32[8,32,4,128]{3,0,2,1:T(8,128)S(1)} %get-tuple-element.336, s32[]{:T(128)S(6)} %copy.127), kind=kOutput, calls=%fused_computation.1.clone.1 | convolution fusion | flops 25165824 | bytes 8519684 | tf_op jit(solution)/shard_map/while/body/eval_jaxpr/shkv,shk->shv/dot_general | solution.py:52
  186.3 10.5 %add_select_fusion.4 = f32[32,4,128,128]{3,2,1,0:T(8,128)} fusion(f32[32,4,128,128]{3,2,1,0:T(8,128)} %get-tuple-element.320, f32[32,4,128]{2,1,0:T(4,128)S(1)} %bitcast.274, f32[32,4,128]{2,1,0:T(4,128)S(1)} %bitcast.275, f32[32,4,128]{2,1,0:T(4,128)S(1)} %exponential_bitcast_fusion.4, pred[32]{0:T(512)(128)(4,1)S(1)} %dynamic-slice_bitcast_fusion.4), kind=kLoop, calls=%fused_computation.clone.1 | loop fusion | flops 8388608 | bytes 16973856 | tf_op jit(solution)/shard_map/while/body/eval_jaxpr/jit(_where)/select_n | solution.py:51
  196.9 9.5 %convolution_bitcast_fusion.4 = f32[1,32,4,128]{3,0,2,1:T(1,128)S(1)} fusion(f32[32,4,128,128]{3,2,1,0:T(8,128)} %add_select_fusion.4, f32[8,32,4,128]{3,0,2,1:T(8,128)S(1)} %get-tuple-element.336, s32[]{:T(128)S(6)} %copy.127), kind=kOutput, calls=%fused_computation.1.clone.1 | convolution fusion | flops 25165824 | bytes 8519684 | tf_op jit(solution)/shard_map/while/body/eval_jaxpr/shkv,shk->shv/dot_general | solution.py:52
  209.2 10.5 %add_select_fusion.4 = f32[32,4,128,128]{3,2,1,0:T(8,128)} fusion(f32[32,4,128,128]{3,2,1,0:T(8,128)} %get-tuple-element.320, f32[32,4,128]{2,1,0:T(4,128)S(1)} %bitcast.274, f32[32,4,128]{2,1,0:T(4,128)S(1)} %bitcast.275, f32[32,4,128]{2,1,0:T(4,128)S(1)} %exponential_bitcast_fusion.4, pred[32]{0:T(512)(128)(4,1)S(1)} %dynamic-slice_bitcast_fusion.4), kind=kLoop, calls=%fused_computation.clone.1 | loop fusion | flops 8388608 | bytes 16973856 | tf_op jit(solution)/shard_map/while/body/eval_jaxpr/jit(_where)/select_n | solution.py:51
  219.7 9.5 %convolution_bitcast_fusion.4 = f32[1,32,4,128]{3,0,2,1:T(1,128)S(1)} fusion(f32[32,4,128,128]{3,2,1,0:T(8,128)} %add_select_fusion.4, f32[8,32,4,128]{3,0,2,1:T(8,128)S(1)} %get-tuple-element.336, s32[]{:T(128)S(6)} %copy.127), kind=kOutput, calls=%fused_computation.1.clone.1 | convolution fusion | flops 25165824 | bytes 8519684 | tf_op jit(solution)/shard_map/while/body/eval_jaxpr/shkv,shk->shv/dot_general | solution.py:52
  232.1 10.5 %add_select_fusion.4 = f32[32,4,128,128]{3,2,1,0:T(8,128)} fusion(f32[32,4,128,128]{3,2,1,0:T(8,128)} %get-tuple-element.320, f32[32,4,128]{2,1,0:T(4,128)S(1)} %bitcast.274, f32[32,4,128]{2,1,0:T(4,128)S(1)} %bitcast.275, f32[32,4,128]{2,1,0:T(4,128)S(1)} %exponential_bitcast_fusion.4, pred[32]{0:T(512)(128)(4,1)S(1)} %dynamic-slice_bitcast_fusion.4), kind=kLoop, calls=%fused_computation.clone.1 | loop fusion | flops 8388608 | bytes 16973856 | tf_op jit(solution)/shard_map/while/body/eval_jaxpr/jit(_where)/select_n | solution.py:51
  242.6 9.5 %convolution_bitcast_fusion.4 = f32[1,32,4,128]{3,0,2,1:T(1,128)S(1)} fusion(f32[32,4,128,128]{3,2,1,0:T(8,128)} %add_select_fusion.4, f32[8,32,4,128]{3,0,2,1:T(8,128)S(1)} %get-tuple-element.336, s32[]{:T(128)S(6)} %copy.127), kind=kOutput, calls=%fused_computation.1.clone.1 | convolution fusion | flops 25165824 | bytes 8519684 | tf_op jit(solution)/shard_map/while/body/eval_jaxpr/shkv,shk->shv/dot_general | solution.py:52
  255.0 16.8 %all-gather.3.cloned.1.call-done = bf16[1024,512]{1,0:T(8,128)(2,1)} async-done(((bf16[256,512]{1,0:T(8,128)(2,1)}), bf16[1024,512]{1,0:T(8,128)(2,1)}) %all-gather.3.cloned.1.call-update) | async-done | bytes 1048592 | tf_op jit(solution)/shard_map/all_gather | solution.py:142
  271.8 4.1 convolution_convert_fusion.1
  276.2 102.2 %all-reduce.3.cloned.1.call-done = bf16[1024,1024]{1,0:T(8,128)(2,1)} async-done(((bf16[1024,1024]{1,0:T(8,128)(2,1)}), bf16[1024,1024]{1,0:T(8,128)(2,1)}) %all-reduce.3.cloned.1.call-update) | async-done | bytes 2097168 | tf_op jit(solution)/shard_map/psum | solution.py:146
  391.1 6.1 psum.30
  397.4 37.4 %reduce-scatter.5.cloned.1.call-done = bf16[256,2048]{0,1:T(8,128)(2,1)} async-done(((bf16[1024,2048]{0,1:T(8,128)(2,1)}), bf16[256,2048]{0,1:T(8,128)(2,1)}) %reduce-scatter.5.cloned.1.call-update) | async-done | bytes 1048592 | tf_op jit(solution)/shard_map/reduce_scatter | solution.py:117
  449.4 191.7 %while.25 = (s32[]{:T(128)}, f32[32,4,128,128]{3,2,1,0:T(8,128)}, f32[8,32,4,128]{3,0,2,1:T(8,128)S(1)}, pred[8,32]{1,0:T(8,128)(4,1)S(1)}, f32[8,32,4,128]{3,0,...) while((s32[]{:T(128)}, f32[32,4,128,128]{3,2,1,0:T(8,128)}, ...), condition=%wide.region_11.12_spmd, body=%wide.region_10.11_spmd.sunk | while | flops 33554432 | bytes 26149088 | solution.py:55
  451.9 10.6 %add_select_fusion.5 = f32[32,4,128,128]{3,2,1,0:T(8,128)} fusion(f32[32,4,128,128]{3,2,1,0:T(8,128)} %get-tuple-element.350, f32[32,4,128]{2,1,0:T(4,128)S(1)} %bitcast.276, f32[32,4,128]{2,1,0:T(4,128)S(1)} %bitcast.277, f32[32,4,128]{2,1,0:T(4,128)S(1)} %exponential_bitcast_fusion.5, pred[32]{0:T(512)(128)(4,1)S(1)} %dynamic-slice_bitcast_fusion.5), kind=kLoop, calls=%fused_computation.10.clone.1 | loop fusion | flops 8388608 | bytes 16973856 | tf_op jit(solution)/shard_map/while/body/eval_jaxpr/jit(_where)/select_n | solution.py:51
  462.4 9.6 %convolution_bitcast_fusion.5 = f32[1,32,4,128]{3,0,2,1:T(1,128)S(1)} fusion(f32[32,4,128,128]{3,2,1,0:T(8,128)} %add_select_fusion.5, f32[8,32,4,128]{3,0,2,1:T(8,128)} %get-tuple-element.366, s32[]{:T(128)S(6)} %copy.137), kind=kOutput, calls=%fused_computation.11.clone.1 | convolution fusion | flops 25165824 | bytes 8519684 | tf_op jit(solution)/shard_map/while/body/eval_jaxpr/shkv,shk->shv/dot_general | solution.py:52
  475.8 10.6 %add_select_fusion.5 = f32[32,4,128,128]{3,2,1,0:T(8,128)} fusion(f32[32,4,128,128]{3,2,1,0:T(8,128)} %get-tuple-element.350, f32[32,4,128]{2,1,0:T(4,128)S(1)} %bitcast.276, f32[32,4,128]{2,1,0:T(4,128)S(1)} %bitcast.277, f32[32,4,128]{2,1,0:T(4,128)S(1)} %exponential_bitcast_fusion.5, pred[32]{0:T(512)(128)(4,1)S(1)} %dynamic-slice_bitcast_fusion.5), kind=kLoop, calls=%fused_computation.10.clone.1 | loop fusion | flops 8388608 | bytes 16973856 | tf_op jit(solution)/shard_map/while/body/eval_jaxpr/jit(_where)/select_n | solution.py:51
  486.4 9.6 %convolution_bitcast_fusion.5 = f32[1,32,4,128]{3,0,2,1:T(1,128)S(1)} fusion(f32[32,4,128,128]{3,2,1,0:T(8,128)} %add_select_fusion.5, f32[8,32,4,128]{3,0,2,1:T(8,128)} %get-tuple-element.366, s32[]{:T(128)S(6)} %copy.137), kind=kOutput, calls=%fused_computation.11.clone.1 | convolution fusion | flops 25165824 | bytes 8519684 | tf_op jit(solution)/shard_map/while/body/eval_jaxpr/shkv,shk->shv/dot_general | solution.py:52
  499.8 10.6 %add_select_fusion.5 = f32[32,4,128,128]{3,2,1,0:T(8,128)} fusion(f32[32,4,128,128]{3,2,1,0:T(8,128)} %get-tuple-element.350, f32[32,4,128]{2,1,0:T(4,128)S(1)} %bitcast.276, f32[32,4,128]{2,1,0:T(4,128)S(1)} %bitcast.277, f32[32,4,128]{2,1,0:T(4,128)S(1)} %exponential_bitcast_fusion.5, pred[32]{0:T(512)(128)(4,1)S(1)} %dynamic-slice_bitcast_fusion.5), kind=kLoop, calls=%fused_computation.10.clone.1 | loop fusion | flops 8388608 | bytes 16973856 | tf_op jit(solution)/shard_map/while/body/eval_jaxpr/jit(_where)/select_n | solution.py:51
  510.4 9.6 %convolution_bitcast_fusion.5 = f32[1,32,4,128]{3,0,2,1:T(1,128)S(1)} fusion(f32[32,4,128,128]{3,2,1,0:T(8,128)} %add_select_fusion.5, f32[8,32,4,128]{3,0,2,1:T(8,128)} %get-tuple-element.366, s32[]{:T(128)S(6)} %copy.137), kind=kOutput, calls=%fused_computation.11.clone.1 | convolution fusion | flops 25165824 | bytes 8519684 | tf_op jit(solution)/shard_map/while/body/eval_jaxpr/shkv,shk->shv/dot_general | solution.py:52
  523.7 10.6 %add_select_fusion.5 = f32[32,4,128,128]{3,2,1,0:T(8,128)} fusion(f32[32,4,128,128]{3,2,1,0:T(8,128)} %get-tuple-element.350, f32[32,4,128]{2,1,0:T(4,128)S(1)} %bitcast.276, f32[32,4,128]{2,1,0:T(4,128)S(1)} %bitcast.277, f32[32,4,128]{2,1,0:T(4,128)S(1)} %exponential_bitcast_fusion.5, pred[32]{0:T(512)(128)(4,1)S(1)} %dynamic-slice_bitcast_fusion.5), kind=kLoop, calls=%fused_computation.10.clone.1 | loop fusion | flops 8388608 | bytes 16973856 | tf_op jit(solution)/shard_map/while/body/eval_jaxpr/jit(_where)/select_n | solution.py:51
  534.3 9.6 %convolution_bitcast_fusion.5 = f32[1,32,4,128]{3,0,2,1:T(1,128)S(1)} fusion(f32[32,4,128,128]{3,2,1,0:T(8,128)} %add_select_fusion.5, f32[8,32,4,128]{3,0,2,1:T(8,128)} %get-tuple-element.366, s32[]{:T(128)S(6)} %copy.137), kind=kOutput, calls=%fused_computation.11.clone.1 | convolution fusion | flops 25165824 | bytes 8519684 | tf_op jit(solution)/shard_map/while/body/eval_jaxpr/shkv,shk->shv/dot_general | solution.py:52
  547.7 10.6 %add_select_fusion.5 = f32[32,4,128,128]{3,2,1,0:T(8,128)} fusion(f32[32,4,128,128]{3,2,1,0:T(8,128)} %get-tuple-element.350, f32[32,4,128]{2,1,0:T(4,128)S(1)} %bitcast.276, f32[32,4,128]{2,1,0:T(4,128)S(1)} %bitcast.277, f32[32,4,128]{2,1,0:T(4,128)S(1)} %exponential_bitcast_fusion.5, pred[32]{0:T(512)(128)(4,1)S(1)} %dynamic-slice_bitcast_fusion.5), kind=kLoop, calls=%fused_computation.10.clone.1 | loop fusion | flops 8388608 | bytes 16973856 | tf_op jit(solution)/shard_map/while/body/eval_jaxpr/jit(_where)/select_n | solution.py:51
  558.3 9.6 %convolution_bitcast_fusion.5 = f32[1,32,4,128]{3,0,2,1:T(1,128)S(1)} fusion(f32[32,4,128,128]{3,2,1,0:T(8,128)} %add_select_fusion.5, f32[8,32,4,128]{3,0,2,1:T(8,128)} %get-tuple-element.366, s32[]{:T(128)S(6)} %copy.137), kind=kOutput, calls=%fused_computation.11.clone.1 | convolution fusion | flops 25165824 | bytes 8519684 | tf_op jit(solution)/shard_map/while/body/eval_jaxpr/shkv,shk->shv/dot_general | solution.py:52
  571.7 10.6 %add_select_fusion.5 = f32[32,4,128,128]{3,2,1,0:T(8,128)} fusion(f32[32,4,128,128]{3,2,1,0:T(8,128)} %get-tuple-element.350, f32[32,4,128]{2,1,0:T(4,128)S(1)} %bitcast.276, f32[32,4,128]{2,1,0:T(4,128)S(1)} %bitcast.277, f32[32,4,128]{2,1,0:T(4,128)S(1)} %exponential_bitcast_fusion.5, pred[32]{0:T(512)(128)(4,1)S(1)} %dynamic-slice_bitcast_fusion.5), kind=kLoop, calls=%fused_computation.10.clone.1 | loop fusion | flops 8388608 | bytes 16973856 | tf_op jit(solution)/shard_map/while/body/eval_jaxpr/jit(_where)/select_n | solution.py:51
  582.2 9.6 %convolution_bitcast_fusion.5 = f32[1,32,4,128]{3,0,2,1:T(1,128)S(1)} fusion(f32[32,4,128,128]{3,2,1,0:T(8,128)} %add_select_fusion.5, f32[8,32,4,128]{3,0,2,1:T(8,128)} %get-tuple-element.366, s32[]{:T(128)S(6)} %copy.137), kind=kOutput, calls=%fused_computation.11.clone.1 | convolution fusion | flops 25165824 | bytes 8519684 | tf_op jit(solution)/shard_map/while/body/eval_jaxpr/shkv,shk->shv/dot_general | solution.py:52
  595.6 10.6 %add_select_fusion.5 = f32[32,4,128,128]{3,2,1,0:T(8,128)} fusion(f32[32,4,128,128]{3,2,1,0:T(8,128)} %get-tuple-element.350, f32[32,4,128]{2,1,0:T(4,128)S(1)} %bitcast.276, f32[32,4,128]{2,1,0:T(4,128)S(1)} %bitcast.277, f32[32,4,128]{2,1,0:T(4,128)S(1)} %exponential_bitcast_fusion.5, pred[32]{0:T(512)(128)(4,1)S(1)} %dynamic-slice_bitcast_fusion.5), kind=kLoop, calls=%fused_computation.10.clone.1 | loop fusion | flops 8388608 | bytes 16973856 | tf_op jit(solution)/shard_map/while/body/eval_jaxpr/jit(_where)/select_n | solution.py:51
  606.2 9.6 %convolution_bitcast_fusion.5 = f32[1,32,4,128]{3,0,2,1:T(1,128)S(1)} fusion(f32[32,4,128,128]{3,2,1,0:T(8,128)} %add_select_fusion.5, f32[8,32,4,128]{3,0,2,1:T(8,128)} %get-tuple-element.366, s32[]{:T(128)S(6)} %copy.137), kind=kOutput, calls=%fused_computation.11.clone.1 | convolution fusion | flops 25165824 | bytes 8519684 | tf_op jit(solution)/shard_map/while/body/eval_jaxpr/shkv,shk->shv/dot_general | solution.py:52
  619.6 10.6 %add_select_fusion.5 = f32[32,4,128,128]{3,2,1,0:T(8,128)} fusion(f32[32,4,128,128]{3,2,1,0:T(8,128)} %get-tuple-element.350, f32[32,4,128]{2,1,0:T(4,128)S(1)} %bitcast.276, f32[32,4,128]{2,1,0:T(4,128)S(1)} %bitcast.277, f32[32,4,128]{2,1,0:T(4,128)S(1)} %exponential_bitcast_fusion.5, pred[32]{0:T(512)(128)(4,1)S(1)} %dynamic-slice_bitcast_fusion.5), kind=kLoop, calls=%fused_computation.10.clone.1 | loop fusion | flops 8388608 | bytes 16973856 | tf_op jit(solution)/shard_map/while/body/eval_jaxpr/jit(_where)/select_n | solution.py:51
  630.2 9.6 %convolution_bitcast_fusion.5 = f32[1,32,4,128]{3,0,2,1:T(1,128)S(1)} fusion(f32[32,4,128,128]{3,2,1,0:T(8,128)} %add_select_fusion.5, f32[8,32,4,128]{3,0,2,1:T(8,128)} %get-tuple-element.366, s32[]{:T(128)S(6)} %copy.137), kind=kOutput, calls=%fused_computation.11.clone.1 | convolution fusion | flops 25165824 | bytes 8519684 | tf_op jit(solution)/shard_map/while/body/eval_jaxpr/shkv,shk->shv/dot_general | solution.py:52
  642.5 16.8 %all-gather.5.cloned.1.call-done = bf16[1024,512]{1,0:T(8,128)(2,1)} async-done(((bf16[256,512]{1,0:T(8,128)(2,1)}), bf16[1024,512]{1,0:T(8,128)(2,1)}) %all-gather.5.cloned.1.call-update) | async-done | bytes 1048592 | tf_op jit(solution)/shard_map/all_gather | solution.py:142
  659.4 4.1 convolution_convert_fusion
  663.5 11.9 %pad_maximum_fusion = f32[2,32,4,128,128]{4,3,2,1,0:T(8,128)} fusion(f32[1,32,4,128,128]{4,3,2,1,0:T(8,128)} %bitcast.272, f32[1,32,4,128,128]{4,3,2,1,0:T(8,128)} %bitcast.273), kind=kLoop, calls=%fused_computation.20 | loop fusion | flops 4194304 | bytes 33554432 | tf_op jit(solution)/shard_map/stack | solution.py:148
  675.5 90.5 %all-reduce.5.cloned.1.call-done = bf16[1024,1024]{1,0:T(8,128)(2,1)} async-done(((bf16[1024,1024]{1,0:T(8,128)(2,1)}), bf16[1024,1024]{1,0:T(8,128)(2,1)}) %all-reduce.5.cloned.1.call-update) | async-done | bytes 2097168 | tf_op jit(solution)/shard_map/psum | solution.py:146
  765.9 3.9 fusion.11
  (172 shorter events, 96.7 us)
Async XLA Ops:
  7.2 4.5 copy-start
  7.2 58.5 %reduce-scatter.3.cloned.1.call-start = ((), (), s32[]{:S(2)}) async-start(), calls=%async_computation.2 | async-start | bytes 5242880 | tf_op jit(solution)/shard_map/reduce_scatter | solution.py:117
  7.2 4.4 copy-start.5
  11.6 1.6 copy-start.7
  13.2 1.6 copy-start.9
  18.4 0.7 copy-start.1
  18.4 9.8 %copy-start.4 = (s32[32]{0:T(128)S(1)}, s32[32]{0:T(128)}, u32[]{:S(2)}) copy-start(s32[32]{0:T(128)} %param.17) | copy-start | bytes 388
  18.4 9.8 %copy-start.2 = (f32[2,512]{1,0:T(2,128)S(1)}, f32[2,512]{1,0:T(2,128)}, u32[]{:S(2)}) copy-start(f32[2,512]{1,0:T(2,128)} %param.23) | copy-start | bytes 12292
  18.4 9.8 %copy-start.3 = (f32[2,512]{1,0:T(2,128)S(1)}, f32[2,512]{1,0:T(2,128)}, u32[]{:S(2)}) copy-start(f32[2,512]{1,0:T(2,128)} %param.25) | copy-start | bytes 12292
  18.4 253.4 %all-gather.3.cloned.1.call-start = ((), (), s32[]{:S(2)}) async-start(), calls=%async_computation.3 | async-start | bytes 1310720 | tf_op jit(solution)/shard_map/all_gather | solution.py:142
  254.9 123.4 %all-reduce.3.cloned.1.call-start = ((), (), s32[]{:S(2)}) async-start(), calls=%async_computation.4 | async-start | bytes 4194304 | tf_op jit(solution)/shard_map/psum | solution.py:146
  275.9 158.8 %reduce-scatter.5.cloned.1.call-start = ((), (), s32[]{:S(2)}) async-start(), calls=%async_computation.5 | async-start | bytes 5242880 | tf_op jit(solution)/shard_map/reduce_scatter | solution.py:117
  381.4 2.7 copy-start.6
  384.1 1.6 copy-start.8
  385.7 1.6 copy-start.10
  390.9 268.5 %all-gather.5.cloned.1.call-start = ((), (), s32[]{:S(2)}) async-start(), calls=%async_computation.6 | async-start | bytes 1310720 | tf_op jit(solution)/shard_map/all_gather | solution.py:142
  642.5 123.4 %all-reduce.5.cloned.1.call-start = ((), (), s32[]{:S(2)}) async-start(), calls=%async_computation.7 | async-start | bytes 4194304 | tf_op jit(solution)/shard_map/psum | solution.py:146
Sparse Core Ops, SparseCore 0:
  18.5 47.1 reduce-scatter.2
  255.1 16.6 all-gather.2
  276.1 102.2 all-reduce.2
  391.0 43.6 reduce-scatter.4
  642.6 16.7 all-gather.4
  663.6 102.2 all-reduce.4
where the time goes:
time: 781 us; the launch traced here: 777 us
  waiting for transfers between devices  289 us (37%)
  other arithmetic  205 us (26%)
  matrix products  175 us (22%)
  local copies, waits for them, and re-layouts  77.5 us (10%)
  blocking collectives  14.5 us (2%)
  between operations  14.5 us (2%)
    psum x2, waiting for transfers between devices, local(): update = lax.psum(partial_value.astype(jnp.bfloat16), 'tp')  193 us
    select_n x16, other arithmetic, advance(): matrix = jnp.where(live_now[:, None, None, None], updated, matrix)  169 us
    dot_general x16, matrix products, advance(): jnp.einsum('shkv,shk->shv', matrix, query_now, precision=lax.Precision.HI...  153 us
    reduce_scatter x2, waiting for transfers between devices, local(): lax.psum_scatter(project().astype(jnp.bfloat16), 'dp', scatter_dimension=...  62.5 us
    all_gather x2, waiting for transfers between devices, local(): lax.all_gather(attention_yields, 'dp', axis=0, tiled=True)  33.6 us
    dynamic_slice x32, local copies, waits for them, and re-layouts, update_tick(): lax.scan(advance, memory_grid, (jnp.moveaxis(queries, 1, 0), jnp.moveaxis...  30.5 us
    dynamic_update_slice x16, local copies, waits for them, and re-layouts, update_tick(): lax.scan(advance, memory_grid, (jnp.moveaxis(queries, 1, 0), jnp.moveaxis...  21.2 us
  transfers between devices with their start and end apart: 6, of which 6 were waited for; matrix products, arithmetic and copies ran while one was open for 3% of the time, Pallas kernels for 0%

commit v1 on v0

--- a/solution.py
+++ b/solution.py
@@ -143,7 +143,7 @@
             out_weight,
             preferred_element_type=jnp.float32,
         )
-        update = lax.psum(partial_value.astype(jnp.bfloat16), "tp")
+        update = jnp.sum(lax.all_gather(partial_value.astype(jnp.bfloat16), "tp"), axis=0)
         residual = (current + update.astype(jnp.float32)).astype(jnp.bfloat16)
     return (residual, jnp.stack(finals))
 

time: 781 us -> 1050 us (1.34)
  waiting for transfers between devices: 289 us -> 537 us
  other arithmetic: 205 us -> 227 us
    all_gather x0 -> x2, waiting for transfers between devices: none -> 442 us  [local(): lax.all_gather(partial_value.astype(jnp.bfloat16), 'tp')]
    psum x2 -> x0, waiting for transfers between devices: 193 us -> none  [local(): update = lax.psum(partial_value.astype(jnp.bfloat16), 'tp')]
    reduce_sum x0 -> x2, other arithmetic: none -> 21.6 us  [local(): jnp.sum(lax.all_gather(partial_value.astype(jnp.bfloat16), 'tp'), axis=0)]
where the time goes in v1:
time: 1050 us; the launch traced here: 1040 us
  waiting for transfers between devices  537 us (51%)
  other arithmetic  227 us (22%)
  matrix products  173 us (16%)
  local copies, waits for them, and re-layouts  76.6 us (7%)
  between operations  14.5 us (1%)
  blocking collectives  14.2 us (1%)
    all_gather x2, waiting for transfers between devices, local(): lax.all_gather(partial_value.astype(jnp.bfloat16), 'tp')  442 us
    select_n x16, other arithmetic, advance(): matrix = jnp.where(live_now[:, None, None, None], updated, matrix)  169 us
    dot_general x16, matrix products, advance(): jnp.einsum('shkv,shk->shv', matrix, query_now, precision=lax.Precision.HI...  153 us
    reduce_scatter x2, waiting for transfers between devices, local(): lax.psum_scatter(project().astype(jnp.bfloat16), 'dp', scatter_dimension=...  61.7 us
    all_gather x2, waiting for transfers between devices, local(): lax.all_gather(attention_yields, 'dp', axis=0, tiled=True)  33.6 us
    dynamic_slice x32, local copies, waits for them, and re-layouts, update_tick(): lax.scan(advance, memory_grid, (jnp.moveaxis(queries, 1, 0), jnp.moveaxis...  30.3 us
    reduce_sum x2, other arithmetic, local(): jnp.sum(lax.all_gather(partial_value.astype(jnp.bfloat16), 'tp'), axis=0)  21.6 us
    dynamic_update_slice x16, local copies, waits for them, and re-layouts, update_tick(): lax.scan(advance, memory_grid, (jnp.moveaxis(queries, 1, 0), jnp.moveaxis...  21.2 us
  transfers between devices with their start and end apart: 6, of which 6 were waited for; matrix products, arithmetic and copies ran while one was open for 3% of the time, Pallas kernels for 0%

profile of v1, /device:TPU:0, one launch (start us, length us, event | category | flops | bytes accessed | tf_op | source)
XLA Modules:
  0.0 1044.4 jit_solution(7309870781674250318)
XLA Ops:
  19.7 8.4 psum.14
  28.3 12.2 %slice_bitcast_fusion = (f32[32,4,128,128]{3,2,1,0:T(8,128)}, f32[32,4,128,128]{3,2,1,0:T(8,128)}) fusion(f32[2,32,4,128,128]{4,3,2,1,0:T(8,128)} %param.27), kind=kLoop, calls=%fused_computation.21 | loop fusion | bytes 33554432 | tf_op jit(solution)/shard_map/squeeze | solution.py:137
  40.6 25.1 %reduce-scatter.3.cloned.1.call-done = bf16[256,2048]{0,1:T(8,128)(2,1)} async-done(((bf16[1024,2048]{0,1:T(8,128)(2,1)}), bf16[256,2048]{0,1:T(8,128)(2,1)}) %reduce-scatter.3.cloned.1.call-update) | async-done | bytes 1048592 | tf_op jit(solution)/shard_map/reduce_scatter | solution.py:117
  70.5 182.8 %while.24 = (s32[]{:T(128)}, f32[32,4,128,128]{3,2,1,0:T(8,128)}, f32[8,32,4,128]{3,0,2,1:T(8,128)S(1)}, pred[8,32]{1,0:T(8,128)(4,1)S(1)}, f32[8,32,4,128]{3,0,...) while((s32[]{:T(128)}, f32[32,4,128,128]{3,2,1,0:T(8,128)}, ...), condition=%wide.region_4.5_spmd, body=%wide.region_3.4_spmd.sunk | while | flops 33554432 | bytes 26149088 | solution.py:55
  71.9 10.5 %add_select_fusion.4 = f32[32,4,128,128]{3,2,1,0:T(8,128)} fusion(f32[32,4,128,128]{3,2,1,0:T(8,128)} %get-tuple-element.320, f32[32,4,128]{2,1,0:T(4,128)S(1)} %bitcast.278, f32[32,4,128]{2,1,0:T(4,128)S(1)} %bitcast.279, f32[32,4,128]{2,1,0:T(4,128)S(1)} %exponential_bitcast_fusion.4, pred[32]{0:T(512)(128)(4,1)S(1)} %dynamic-slice_bitcast_fusion.4), kind=kLoop, calls=%fused_computation.clone.1 | loop fusion | flops 8388608 | bytes 16973856 | tf_op jit(solution)/shard_map/while/body/eval_jaxpr/jit(_where)/select_n | solution.py:51
  82.5 9.5 convolution_bitcast_fusion.4
  94.8 10.5 %add_select_fusion.4 = f32[32,4,128,128]{3,2,1,0:T(8,128)} fusion(f32[32,4,128,128]{3,2,1,0:T(8,128)} %get-tuple-element.320, f32[32,4,128]{2,1,0:T(4,128)S(1)} %bitcast.278, f32[32,4,128]{2,1,0:T(4,128)S(1)} %bitcast.279, f32[32,4,128]{2,1,0:T(4,128)S(1)} %exponential_bitcast_fusion.4, pred[32]{0:T(512)(128)(4,1)S(1)} %dynamic-slice_bitcast_fusion.4), kind=kLoop, calls=%fused_computation.clone.1 | loop fusion | flops 8388608 | bytes 16973856 | tf_op jit(solution)/shard_map/while/body/eval_jaxpr/jit(_where)/select_n | solution.py:51
  105.3 9.5 convolution_bitcast_fusion.4
  117.6 10.5 %add_select_fusion.4 = f32[32,4,128,128]{3,2,1,0:T(8,128)} fusion(f32[32,4,128,128]{3,2,1,0:T(8,128)} %get-tuple-element.320, f32[32,4,128]{2,1,0:T(4,128)S(1)} %bitcast.278, f32[32,4,128]{2,1,0:T(4,128)S(1)} %bitcast.279, f32[32,4,128]{2,1,0:T(4,128)S(1)} %exponential_bitcast_fusion.4, pred[32]{0:T(512)(128)(4,1)S(1)} %dynamic-slice_bitcast_fusion.4), kind=kLoop, calls=%fused_computation.clone.1 | loop fusion | flops 8388608 | bytes 16973856 | tf_op jit(solution)/shard_map/while/body/eval_jaxpr/jit(_where)/select_n | solution.py:51
  128.2 9.5 convolution_bitcast_fusion.4
  140.5 10.5 %add_select_fusion.4 = f32[32,4,128,128]{3,2,1,0:T(8,128)} fusion(f32[32,4,128,128]{3,2,1,0:T(8,128)} %get-tuple-element.320, f32[32,4,128]{2,1,0:T(4,128)S(1)} %bitcast.278, f32[32,4,128]{2,1,0:T(4,128)S(1)} %bitcast.279, f32[32,4,128]{2,1,0:T(4,128)S(1)} %exponential_bitcast_fusion.4, pred[32]{0:T(512)(128)(4,1)S(1)} %dynamic-slice_bitcast_fusion.4), kind=kLoop, calls=%fused_computation.clone.1 | loop fusion | flops 8388608 | bytes 16973856 | tf_op jit(solution)/shard_map/while/body/eval_jaxpr/jit(_where)/select_n | solution.py:51
  151.0 9.5 convolution_bitcast_fusion.4
  163.3 10.5 %add_select_fusion.4 = f32[32,4,128,128]{3,2,1,0:T(8,128)} fusion(f32[32,4,128,128]{3,2,1,0:T(8,128)} %get-tuple-element.320, f32[32,4,128]{2,1,0:T(4,128)S(1)} %bitcast.278, f32[32,4,128]{2,1,0:T(4,128)S(1)} %bitcast.279, f32[32,4,128]{2,1,0:T(4,128)S(1)} %exponential_bitcast_fusion.4, pred[32]{0:T(512)(128)(4,1)S(1)} %dynamic-slice_bitcast_fusion.4), kind=kLoop, calls=%fused_computation.clone.1 | loop fusion | flops 8388608 | bytes 16973856 | tf_op jit(solution)/shard_map/while/body/eval_jaxpr/jit(_where)/select_n | solution.py:51
  173.9 9.5 convolution_bitcast_fusion.4
  186.2 10.5 %add_select_fusion.4 = f32[32,4,128,128]{3,2,1,0:T(8,128)} fusion(f32[32,4,128,128]{3,2,1,0:T(8,128)} %get-tuple-element.320, f32[32,4,128]{2,1,0:T(4,128)S(1)} %bitcast.278, f32[32,4,128]{2,1,0:T(4,128)S(1)} %bitcast.279, f32[32,4,128]{2,1,0:T(4,128)S(1)} %exponential_bitcast_fusion.4, pred[32]{0:T(512)(128)(4,1)S(1)} %dynamic-slice_bitcast_fusion.4), kind=kLoop, calls=%fused_computation.clone.1 | loop fusion | flops 8388608 | bytes 16973856 | tf_op jit(solution)/shard_map/while/body/eval_jaxpr/jit(_where)/select_n | solution.py:51
  196.7 9.5 convolution_bitcast_fusion.4
  209.0 10.5 %add_select_fusion.4 = f32[32,4,128,128]{3,2,1,0:T(8,128)} fusion(f32[32,4,128,128]{3,2,1,0:T(8,128)} %get-tuple-element.320, f32[32,4,128]{2,1,0:T(4,128)S(1)} %bitcast.278, f32[32,4,128]{2,1,0:T(4,128)S(1)} %bitcast.279, f32[32,4,128]{2,1,0:T(4,128)S(1)} %exponential_bitcast_fusion.4, pred[32]{0:T(512)(128)(4,1)S(1)} %dynamic-slice_bitcast_fusion.4), kind=kLoop, calls=%fused_computation.clone.1 | loop fusion | flops 8388608 | bytes 16973856 | tf_op jit(solution)/shard_map/while/body/eval_jaxpr/jit(_where)/select_n | solution.py:51
  219.6 9.5 convolution_bitcast_fusion.4
  231.9 10.5 %add_select_fusion.4 = f32[32,4,128,128]{3,2,1,0:T(8,128)} fusion(f32[32,4,128,128]{3,2,1,0:T(8,128)} %get-tuple-element.320, f32[32,4,128]{2,1,0:T(4,128)S(1)} %bitcast.278, f32[32,4,128]{2,1,0:T(4,128)S(1)} %bitcast.279, f32[32,4,128]{2,1,0:T(4,128)S(1)} %exponential_bitcast_fusion.4, pred[32]{0:T(512)(128)(4,1)S(1)} %dynamic-slice_bitcast_fusion.4), kind=kLoop, calls=%fused_computation.clone.1 | loop fusion | flops 8388608 | bytes 16973856 | tf_op jit(solution)/shard_map/while/body/eval_jaxpr/jit(_where)/select_n | solution.py:51
  242.4 9.5 convolution_bitcast_fusion.4
  254.8 16.8 %all-gather.7.cloned.1.call-done = bf16[1024,512]{1,0:T(8,128)(2,1)} async-done(((bf16[256,512]{1,0:T(8,128)(2,1)}), bf16[1024,512]{1,0:T(8,128)(2,1)}) %all-gather.7.cloned.1.call-update) | async-done | bytes 1048592 | tf_op jit(solution)/shard_map/all_gather | solution.py:142
  271.6 4.1 convolution_convert_fusion.1
  276.0 227.2 %all-gather.11.cloned.1.call-done = bf16[8192,1024]{1,0:T(8,128)(2,1)} async-done(((bf16[1024,1024]{1,0:T(8,128)(2,1)}), bf16[8192,1024]{1,0:T(8,128)(2,1)}) %all-gather.11.cloned.1.call-update) | async-done | bytes 16777232 | tf_op jit(solution)/shard_map/all_gather | solution.py:146
  503.2 10.8 %reduce_sum.62 = bf16[1024,1024]{1,0:T(8,128)(2,1)} reduce(bf16[8,1024,1024]{2,1,0:T(8,128)(2,1)} %bitcast.277, bf16[]{:T(256)} %constant.59.clone.1), dimensions={0}, to_apply=%region_6.7 | reduce | flops 7340032 | bytes 18874370 | tf_op jit(solution)/shard_map/reduce_sum | solution.py:146
  525.7 5.9 psum.15
  531.7 36.6 %reduce-scatter.5.cloned.1.call-done = bf16[256,2048]{0,1:T(8,128)(2,1)} async-done(((bf16[1024,2048]{0,1:T(8,128)(2,1)}), bf16[256,2048]{0,1:T(8,128)(2,1)}) %reduce-scatter.5.cloned.1.call-update) | async-done | bytes 1048592 | tf_op jit(solution)/shard_map/reduce_scatter | solution.py:117
  581.1 191.9 %while.25 = (s32[]{:T(128)}, f32[32,4,128,128]{3,2,1,0:T(8,128)}, f32[8,32,4,128]{3,0,2,1:T(8,128)S(1)}, pred[8,32]{1,0:T(8,128)(4,1)S(1)}, f32[8,32,4,128]{3,0,...) while((s32[]{:T(128)}, f32[32,4,128,128]{3,2,1,0:T(8,128)}, ...), condition=%wide.region_11.12_spmd, body=%wide.region_10.11_spmd.sunk | while | flops 33554432 | bytes 26149088 | solution.py:55
  583.6 10.6 %add_select_fusion.5 = f32[32,4,128,128]{3,2,1,0:T(8,128)} fusion(f32[32,4,128,128]{3,2,1,0:T(8,128)} %get-tuple-element.350, f32[32,4,128]{2,1,0:T(4,128)S(1)} %bitcast.280, f32[32,4,128]{2,1,0:T(4,128)S(1)} %bitcast.281, f32[32,4,128]{2,1,0:T(4,128)S(1)} %exponential_bitcast_fusion.5, pred[32]{0:T(512)(128)(4,1)S(1)} %dynamic-slice_bitcast_fusion.5), kind=kLoop, calls=%fused_computation.10.clone.1 | loop fusion | flops 8388608 | bytes 16973856 | tf_op jit(solution)/shard_map/while/body/eval_jaxpr/jit(_where)/select_n | solution.py:51
  594.2 9.6 convolution_bitcast_fusion.5
  607.6 10.6 %add_select_fusion.5 = f32[32,4,128,128]{3,2,1,0:T(8,128)} fusion(f32[32,4,128,128]{3,2,1,0:T(8,128)} %get-tuple-element.350, f32[32,4,128]{2,1,0:T(4,128)S(1)} %bitcast.280, f32[32,4,128]{2,1,0:T(4,128)S(1)} %bitcast.281, f32[32,4,128]{2,1,0:T(4,128)S(1)} %exponential_bitcast_fusion.5, pred[32]{0:T(512)(128)(4,1)S(1)} %dynamic-slice_bitcast_fusion.5), kind=kLoop, calls=%fused_computation.10.clone.1 | loop fusion | flops 8388608 | bytes 16973856 | tf_op jit(solution)/shard_map/while/body/eval_jaxpr/jit(_where)/select_n | solution.py:51
  618.2 9.6 convolution_bitcast_fusion.5
  631.6 10.6 %add_select_fusion.5 = f32[32,4,128,128]{3,2,1,0:T(8,128)} fusion(f32[32,4,128,128]{3,2,1,0:T(8,128)} %get-tuple-element.350, f32[32,4,128]{2,1,0:T(4,128)S(1)} %bitcast.280, f32[32,4,128]{2,1,0:T(4,128)S(1)} %bitcast.281, f32[32,4,128]{2,1,0:T(4,128)S(1)} %exponential_bitcast_fusion.5, pred[32]{0:T(512)(128)(4,1)S(1)} %dynamic-slice_bitcast_fusion.5), kind=kLoop, calls=%fused_computation.10.clone.1 | loop fusion | flops 8388608 | bytes 16973856 | tf_op jit(solution)/shard_map/while/body/eval_jaxpr/jit(_where)/select_n | solution.py:51
  642.2 9.6 convolution_bitcast_fusion.5
  655.6 10.6 %add_select_fusion.5 = f32[32,4,128,128]{3,2,1,0:T(8,128)} fusion(f32[32,4,128,128]{3,2,1,0:T(8,128)} %get-tuple-element.350, f32[32,4,128]{2,1,0:T(4,128)S(1)} %bitcast.280, f32[32,4,128]{2,1,0:T(4,128)S(1)} %bitcast.281, f32[32,4,128]{2,1,0:T(4,128)S(1)} %exponential_bitcast_fusion.5, pred[32]{0:T(512)(128)(4,1)S(1)} %dynamic-slice_bitcast_fusion.5), kind=kLoop, calls=%fused_computation.10.clone.1 | loop fusion | flops 8388608 | bytes 16973856 | tf_op jit(solution)/shard_map/while/body/eval_jaxpr/jit(_where)/select_n | solution.py:51
  666.2 9.6 convolution_bitcast_fusion.5
  679.6 10.6 %add_select_fusion.5 = f32[32,4,128,128]{3,2,1,0:T(8,128)} fusion(f32[32,4,128,128]{3,2,1,0:T(8,128)} %get-tuple-element.350, f32[32,4,128]{2,1,0:T(4,128)S(1)} %bitcast.280, f32[32,4,128]{2,1,0:T(4,128)S(1)} %bitcast.281, f32[32,4,128]{2,1,0:T(4,128)S(1)} %exponential_bitcast_fusion.5, pred[32]{0:T(512)(128)(4,1)S(1)} %dynamic-slice_bitcast_fusion.5), kind=kLoop, calls=%fused_computation.10.clone.1 | loop fusion | flops 8388608 | bytes 16973856 | tf_op jit(solution)/shard_map/while/body/eval_jaxpr/jit(_where)/select_n | solution.py:51
  690.2 9.6 convolution_bitcast_fusion.5
  703.6 10.6 %add_select_fusion.5 = f32[32,4,128,128]{3,2,1,0:T(8,128)} fusion(f32[32,4,128,128]{3,2,1,0:T(8,128)} %get-tuple-element.350, f32[32,4,128]{2,1,0:T(4,128)S(1)} %bitcast.280, f32[32,4,128]{2,1,0:T(4,128)S(1)} %bitcast.281, f32[32,4,128]{2,1,0:T(4,128)S(1)} %exponential_bitcast_fusion.5, pred[32]{0:T(512)(128)(4,1)S(1)} %dynamic-slice_bitcast_fusion.5), kind=kLoop, calls=%fused_computation.10.clone.1 | loop fusion | flops 8388608 | bytes 16973856 | tf_op jit(solution)/shard_map/while/body/eval_jaxpr/jit(_where)/select_n | solution.py:51
  714.2 9.6 convolution_bitcast_fusion.5
  727.5 10.6 %add_select_fusion.5 = f32[32,4,128,128]{3,2,1,0:T(8,128)} fusion(f32[32,4,128,128]{3,2,1,0:T(8,128)} %get-tuple-element.350, f32[32,4,128]{2,1,0:T(4,128)S(1)} %bitcast.280, f32[32,4,128]{2,1,0:T(4,128)S(1)} %bitcast.281, f32[32,4,128]{2,1,0:T(4,128)S(1)} %exponential_bitcast_fusion.5, pred[32]{0:T(512)(128)(4,1)S(1)} %dynamic-slice_bitcast_fusion.5), kind=kLoop, calls=%fused_computation.10.clone.1 | loop fusion | flops 8388608 | bytes 16973856 | tf_op jit(solution)/shard_map/while/body/eval_jaxpr/jit(_where)/select_n | solution.py:51
  738.1 9.6 convolution_bitcast_fusion.5
  751.5 10.6 %add_select_fusion.5 = f32[32,4,128,128]{3,2,1,0:T(8,128)} fusion(f32[32,4,128,128]{3,2,1,0:T(8,128)} %get-tuple-element.350, f32[32,4,128]{2,1,0:T(4,128)S(1)} %bitcast.280, f32[32,4,128]{2,1,0:T(4,128)S(1)} %bitcast.281, f32[32,4,128]{2,1,0:T(4,128)S(1)} %exponential_bitcast_fusion.5, pred[32]{0:T(512)(128)(4,1)S(1)} %dynamic-slice_bitcast_fusion.5), kind=kLoop, calls=%fused_computation.10.clone.1 | loop fusion | flops 8388608 | bytes 16973856 | tf_op jit(solution)/shard_map/while/body/eval_jaxpr/jit(_where)/select_n | solution.py:51
  762.1 9.6 convolution_bitcast_fusion.5
  774.5 16.8 %all-gather.9.cloned.1.call-done = bf16[1024,512]{1,0:T(8,128)(2,1)} async-done(((bf16[256,512]{1,0:T(8,128)(2,1)}), bf16[1024,512]{1,0:T(8,128)(2,1)}) %all-gather.9.cloned.1.call-update) | async-done | bytes 1048592 | tf_op jit(solution)/shard_map/all_gather | solution.py:142
  791.3 4.1 convolution_convert_fusion
  795.5 12.9 %pad_maximum_fusion = f32[2,32,4,128,128]{4,3,2,1,0:T(8,128)} fusion(f32[1,32,4,128,128]{4,3,2,1,0:T(8,128)} %bitcast.274, f32[1,32,4,128,128]{4,3,2,1,0:T(8,128)} %bitcast.275), kind=kLoop, calls=%fused_computation.20 | loop fusion | flops 4194304 | bytes 33554432 | tf_op jit(solution)/shard_map/stack | solution.py:148
  808.3 214.6 %all-gather.13.cloned.1.call-done = bf16[8192,1024]{1,0:T(8,128)(2,1)} async-done(((bf16[1024,1024]{1,0:T(8,128)(2,1)}), bf16[8192,1024]{1,0:T(8,128)(2,1)}) %all-gather.13.cloned.1.call-update) | async-done | bytes 16777232 | tf_op jit(solution)/shard_map/all_gather | solution.py:146
  1022.9 10.8 %reduce_sum.65 = bf16[1024,1024]{1,0:T(8,128)(2,1)} reduce(bf16[8,1024,1024]{2,1,0:T(8,128)(2,1)} %bitcast.276, bf16[]{:T(256)} %constant.59.clone.1), dimensions={0}, to_apply=%region_13.14 | reduce | flops 7340032 | bytes 18874370 | tf_op jit(solution)/shard_map/reduce_sum | solution.py:146
  (176 shorter events, 101.2 us)
Async XLA Ops:
  7.2 4.5 copy-start
  7.2 58.5 %reduce-scatter.3.cloned.1.call-start = ((), (), s32[]{:S(2)}) async-start(), calls=%async_computation.2 | async-start | bytes 5242880 | tf_op jit(solution)/shard_map/reduce_scatter | solution.py:117
  7.2 4.4 copy-start.5
  11.6 1.6 copy-start.7
  13.2 1.6 copy-start.10
  18.4 0.7 copy-start.1
  18.4 9.8 copy-start.4
  18.4 9.8 copy-start.2
  18.4 9.8 copy-start.3
  18.4 253.2 %all-gather.7.cloned.1.call-start = ((), (), s32[]{:S(2)}) async-start(), calls=%async_computation.3 | async-start | bytes 1310720 | tf_op jit(solution)/shard_map/all_gather | solution.py:142
  254.8 248.4 %all-gather.11.cloned.1.call-start = ((), (), s32[]{:S(2)}) async-start(), calls=%async_computation.6 | async-start | bytes 18874368 | tf_op jit(solution)/shard_map/all_gather | solution.py:146
  275.8 292.5 %reduce-scatter.5.cloned.1.call-start = ((), (), s32[]{:S(2)}) async-start(), calls=%async_computation.4 | async-start | bytes 5242880 | tf_op jit(solution)/shard_map/reduce_scatter | solution.py:117
  514.0 3.2 copy-start.6
  517.2 1.6 copy-start.8
  518.7 1.6 copy-start.9
  520.3 1.6 copy-start.11
  525.5 265.8 %all-gather.9.cloned.1.call-start = ((), (), s32[]{:S(2)}) async-start(), calls=%async_computation.5 | async-start | bytes 1310720 | tf_op jit(solution)/shard_map/all_gather | solution.py:142
  774.5 248.4 %all-gather.13.cloned.1.call-start = ((), (), s32[]{:S(2)}) async-start(), calls=%async_computation.7 | async-start | bytes 18874368 | tf_op jit(solution)/shard_map/all_gather | solution.py:146
Sparse Core Ops, SparseCore 0:
  18.5 47.1 reduce-scatter.2
  254.9 16.6 all-gather.6
  275.9 227.2 all-gather.10
  525.7 42.5 reduce-scatter.4
  774.6 16.6 all-gather.8
  795.6 227.2 all-gather.12
